TPU v7x, 32 devices: a whole 2x2x4 slice. The times are simulated.
32 devices in a mesh: sp: 8 (over z, x), tp: 4 (over y, core).
Axes of the slice: x: 2, y: 2, z: 4, core: 2. Of those that a mesh axis runs over, the one named last changes fastest.
Arguments:
- inputs: bfloat16 [8192, 2048], P('sp'), may hold values from -9 to 9
- w_query: bfloat16 [2048, 1024], P(None, 'tp'), may hold values from -0.15692044 to 0.15692044
- w_key: bfloat16 [2048, 1024], P(None, 'tp'), may hold values from -0.15692044 to 0.15692044
- w_value: bfloat16 [2048, 1024], P(None, 'tp'), may hold values from -0.125 to 0.125
- w_glu_value: bfloat16 [2048, 1024], P(None, 'tp'), may hold values from -0.37565048 to 0.37565048
- w_glu_gate: bfloat16 [2048, 1024], P(None, 'tp'), may hold values from -0.125 to 0.125
- conv_taps: float32 [31, 1024], P(None, 'tp'), may hold values from -4 to 4
- conv_gain: float32 [1024], P('tp'), may hold values from 0.1 to 1.9
- log_forget: float32 [8192, 8], P('sp', 'tp'), may hold values from -8192 to 0, as said below
- w_out: bfloat16 [2048, 2048], replicated, may hold values from -0.125 to 0.125
Outputs:
- result: bfloat16 [8192, 2048], P(('sp', 'tp'))
Inputs may be any that keep to these rules, and one draw needn't show every extreme that they name: `log_forget`: for each head, non-increasing along positions and at most zero.
All inputs are finite; a program needn't handle non-finite values.
Results may differ from a plain program's by a relative error of at most 0.014.
Values may be sent and summed in bfloat16 or wider, within the bound.
A program may use at most 128 MiB of HBM per device.

v0:
```python
import math
import jax
import jax.numpy as jnp
from jax import lax
from jax.sharding import PartitionSpec as P

HEAD_DIM = 128
NORM_EPS = 1e-05


def passed_along(value, axis, steps):
    count = lax.axis_size(axis)
    leading, last = (max(0, -steps), min(count, count - steps))
    return lax.ppermute(value, axis, [(source, source + steps) for source in range(leading, last)])


def on_device(
    inputs,
    w_query,
    w_key,
    w_value,
    w_glu_value,
    w_glu_gate,
    conv_taps,
    conv_gain,
    log_forget,
    w_out,
):
    tok_rows = inputs.shape[0]
    channels = w_glu_value.shape[1]
    heads_here = w_query.shape[1] // HEAD_DIM
    attn_width = heads_here * HEAD_DIM
    tp_count = lax.axis_size("tp")
    tp_place = lax.axis_index("tp")
    total_channels = channels * tp_count
    row_start = lax.axis_index("sp") * tok_rows
    last_row = row_start + tok_rows - 1
    glu_value = jnp.dot(inputs, w_glu_value, preferred_element_type=jnp.float32)
    glu_gate = jnp.dot(inputs, w_glu_gate, preferred_element_type=jnp.float32)
    gated = (glu_value * jax.nn.sigmoid(glu_gate)).astype(jnp.bfloat16)
    kernel = conv_taps.shape[0]
    halo_rows = passed_along(gated[tok_rows - (kernel - 1) :], "sp", 1)
    padded = jnp.concatenate([halo_rows, gated], axis=0).astype(jnp.float32)
    conv_sum = jnp.zeros((tok_rows, channels), jnp.float32)
    for offset in range(kernel):
        conv_sum = conv_sum + conv_taps[offset] * padded[offset : offset + tok_rows]
    mean_value = lax.psum(jnp.sum(conv_sum, axis=1), "tp") / total_channels
    centered = conv_sum - mean_value[:, None]
    spread = lax.psum(jnp.sum(centered * centered, axis=1), "tp") / total_channels
    conv_rows = jax.nn.silu(centered * lax.rsqrt(spread + NORM_EPS)[:, None] * conv_gain).astype(
        jnp.bfloat16
    )
    query_rows = jnp.dot(inputs, w_query, preferred_element_type=jnp.float32).astype(jnp.bfloat16)
    key_rows = jnp.dot(inputs, w_key, preferred_element_type=jnp.float32).astype(jnp.bfloat16)
    value_rows = jnp.dot(inputs, w_value, preferred_element_type=jnp.float32).astype(jnp.bfloat16)
    query_heads = query_rows.reshape(tok_rows, heads_here, HEAD_DIM)
    own_gates = jnp.transpose(log_forget)
    gates_all = lax.all_gather(log_forget, "sp", axis=0, tiled=True)
    score_scale = HEAD_DIM ** (-0.5)
    query_pos = row_start + jnp.arange(tok_rows, dtype=jnp.int32)
    start_state = (
        jnp.full((heads_here, tok_rows), -1e30, jnp.float32),
        jnp.zeros((heads_here, tok_rows), jnp.float32),
        jnp.zeros((heads_here, tok_rows, HEAD_DIM), jnp.float32),
    )
    piece_keys = lax.all_gather(key_rows, "sp", axis=0, tiled=True)
    piece_values = lax.all_gather(value_rows, "sp", axis=0, tiled=True)
    block_rows = math.gcd(piece_keys.shape[0], tok_rows)
    shards = piece_keys.shape[0] // block_rows
    key_iota = jnp.arange(block_rows, dtype=jnp.int32)

    def one_shard(shard_number, carried_state):
        offset = shard_number * block_rows
        key_first = offset

        def attend(state_in):
            running_max, running_sum, running_out = state_in
            shard_keys = lax.dynamic_slice_in_dim(piece_keys, offset, block_rows, 0).reshape(
                block_rows, heads_here, HEAD_DIM
            )
            shard_values = lax.dynamic_slice_in_dim(piece_values, offset, block_rows, 0).reshape(
                block_rows, heads_here, HEAD_DIM
            )
            shard_gates = jnp.transpose(
                lax.dynamic_slice_in_dim(gates_all, key_first, block_rows, 0)
            )
            scores = (
                jnp.einsum(
                    "qhd,khd->hqk", query_heads, shard_keys, preferred_element_type=jnp.float32
                )
                * score_scale
            )
            scores = scores + own_gates[:, :, None] - shard_gates[:, None, :]
            allowed = ((key_first + key_iota)[None, :] <= query_pos[:, None])[None]
            masked = jnp.where(allowed, scores, -1e30)
            new_max = jnp.maximum(running_max, jnp.max(masked, axis=2))
            weights = jnp.where(allowed, jnp.exp(masked - new_max[:, :, None]), 0.0)
            rescale = jnp.exp(running_max - new_max)
            new_sum = running_sum * rescale + jnp.sum(weights, axis=2)
            mixture = jnp.einsum(
                "hqk,khd->hqd",
                weights.astype(jnp.bfloat16),
                shard_values,
                preferred_element_type=jnp.float32,
            )
            new_out = running_out * rescale[:, :, None] + mixture
            return (new_max, new_sum, new_out)

        def keep_state(state_in):
            return state_in

        return lax.cond(key_first <= last_row, attend, keep_state, carried_state)

    final_max, final_sum, final_out = lax.fori_loop(0, shards, one_shard, start_state)
    attn_heads = (final_out / final_sum[:, :, None]).astype(jnp.bfloat16)
    attn_rows = jnp.transpose(attn_heads, (1, 0, 2)).reshape(tok_rows, attn_width)
    conv_weight = lax.dynamic_slice_in_dim(w_out, tp_place * channels, channels, 0)
    attn_weight = lax.dynamic_slice_in_dim(
        w_out, total_channels + tp_place * attn_width, attn_width, 0
    )
    projected = jnp.dot(conv_rows, conv_weight, preferred_element_type=jnp.float32)
    return lax.psum_scatter(
        (projected + jnp.dot(attn_rows, attn_weight, preferred_element_type=jnp.float32)).astype(
            jnp.bfloat16
        ),
        "tp",
        scatter_dimension=0,
        tiled=True,
    )


def solution(mesh):
    in_specs = (
        P("sp", None),
        P(None, "tp"),
        P(None, "tp"),
        P(None, "tp"),
        P(None, "tp"),
        P(None, "tp"),
        P(None, "tp"),
        P("tp"),
        P("sp", "tp"),
        P(),
    )
    out_specs = P(("sp", "tp"), None)
    return jax.shard_map(
        on_device, mesh=mesh, in_specs=in_specs, out_specs=out_specs, check_vma=False
    )
```

profile of v0, /device:TPU:0, one launch (start us, length us, event | category | flops | bytes accessed | tf_op | source)
XLA Modules:
  0.0 321.7 jit_solution(7589455608530308768)
XLA Ops:
  6.5 1.2 copy-done
  7.8 4.2 %convolution_convert_fusion.2 = bf16[1024,256]{1,0:T(8,128)(2,1)} fusion(bf16[1024,2048]{1,0:T(8,128)(2,1)} %param.14, bf16[2048,256]{1,0:T(8,128)(2,1)S(1)} %copy-done), kind=kOutput, calls=%fused_computation.30 | convolution fusion | flops 1074003968 | bytes 5767168 | tf_op jit(solution)/shard_map/dot_general | solution.py:54
  12.1 4.6 %convolution_convert_fusion = bf16[1024,256]{1,0:T(8,128)(2,1)} fusion(bf16[1024,2048]{1,0:T(8,128)(2,1)} %param.14, bf16[2048,256]{1,0:T(8,128)(2,1)} %param.17), kind=kOutput, calls=%fused_computation.28 | convolution fusion | flops 1074003968 | bytes 5767168 | tf_op jit(solution)/shard_map/dot_general | solution.py:55
  16.8 3.6 %fusion.18 = f32[1024,256]{1,0:T(8,128)S(1)} fusion(bf16[1024,2048]{1,0:T(8,128)(2,1)} %param.14, bf16[2048,256]{1,0:T(8,128)(2,1)S(1)} %copy-done.6), kind=kOutput, calls=%fused_computation.26 | convolution fusion | flops 1074528256 | bytes 6291456 | tf_op jit(solution)/shard_map/dot_general | solution.py:39
  20.4 1.3 fusion.19
  21.7 4.9 %collective-permute-start = (bf16[30,256]{1,0:T(8,128)(2,1)S(1)}, bf16[30,256]{1,0:T(8,128)(2,1)S(1)}, u32[]{:S(2)}, u32[]{:S(2)}) collective-permute-start(bf16[30,256]{1,0:T(8,128)(2,1)S(1)} %slice.252), channel_id=1, source_target_pairs={{0,4},{4,8},{8,12},{12,16},{16,20},{20,24},{24,28},{1,5},{5,9},{9,... | collective-permute-start | bytes 46088 | tf_op jit(solution)/shard_map/ppermute | solution.py:14
  26.6 3.8 %convolution_convert_fusion.1 = bf16[1024,256]{0,1:T(8,128)(2,1)S(1)} fusion(bf16[1024,2048]{1,0:T(8,128)(2,1)} %param.14, bf16[2048,256]{1,0:T(8,128)(2,1)} %param.15), kind=kOutput, calls=%fused_computation.29 | convolution fusion | flops 1074003968 | bytes 5767168 | tf_op jit(solution)/shard_map/dot_general | solution.py:53
  30.8 31.8 %all_gather.10 = f32[8192,2]{0,1:T(2,128)S(1)} all-gather(f32[1024,2]{0,1:T(2,128)S(1)} %copy-done.2), channel_id=1, replica_groups=mesh['sp'=8,'tp'=4] {'sp'}, dimensions={0}, use_global_device_ids=true | all-gather | bytes 73728 | tf_op jit(solution)/shard_map/all_gather | solution.py:58
  62.7 4.3 %fusion.60 = (f32[1024]{0:T(1024)S(1)}, f32[1024,256]{1,0:T(8,128)S(1)}) fusion(f32[1054,256]{1,0:T(8,128)S(1)} %maximum_convert_fusion, f32[256]{0:T(256)S(1)} %bitcast.80, f32[256]{0:T(256)S(1)} %bitcast.81, f32[256]{0:T(256)S(1)} %bitcast.83, f32[256]{0:T(256)S(1)} %bitcast.84, f32[256]{0:T(256)S(1)} %bitcast.85, f32[256]{0:T(256)S(1)} %bitcast.86, ...), kind=kLoop, calls=%fused_computation.108 | loop fusion | flops 16251904 | bytes 33590272 | tf_op jit(solution)/shard_map/reduce_sum | solution.py:47
  67.1 6.1 %psum.14 = f32[1024]{0:T(1024)S(1)} all-reduce(f32[1024]{0:T(1024)S(1)} %get-tuple-element.333), channel_id=1, replica_groups=mesh['sp'=8,'tp'=4] {'tp'}, use_global_device_ids=true, to_apply=%region_1.0 | all-reduce | flops 1024 | bytes 8192 | tf_op jit(solution)/shard_map/psum | solution.py:47
  73.5 6.6 %psum.15 = f32[1024]{0:T(1024)S(1)} all-reduce(f32[1024]{0:T(1024)S(1)} %multiply_reduce_fusion), channel_id=1, replica_groups=mesh['sp'=8,'tp'=4] {'tp'}, use_global_device_ids=true, to_apply=%region_3.0 | all-reduce | flops 1024 | bytes 8192 | tf_op jit(solution)/shard_map/psum | solution.py:49
  80.2 5.8 %fusion.51 = f32[1024,2048]{1,0:T(8,128)} fusion(bf16[2048,2048]{1,0:T(8,128)(2,1)} %param.23, s32[]{:T(128)S(6)} %select_n.18, f32[1024,256]{1,0:T(8,128)S(1)} %get-tuple-element.334, f32[256]{0:T(256)S(1)} %copy-done.4, f32[1024]{0:T(1024)S(1)} %add_rsqrt_fusion, f32[1024]{0:T(1024)S(1)} %broadcast_multiply_fusion), kind=kOutput, calls=%fused_computation.94 | convolution fusion | flops 1075838976 | bytes 10494980 | tf_op jit(solution)/shard_map/dot_general | solution.py:121
  86.0 2.5 all-gather.3.cloned.1.call-done
  88.5 6.4 %copy.16 = bf16[8192,256]{0,1:T(8,128)(2,1)} copy(bf16[8192,256]{1,0:T(8,128)(2,1)} %all-gather.3.cloned.1.call-done) | data formatting | bytes 8388608
  94.9 67.2 %all-gather.5.cloned.1.call-done = bf16[8192,256]{1,0:T(8,128)(2,1)} async-done(((bf16[1024,256]{1,0:T(8,128)(2,1)}), bf16[8192,256]{1,0:T(8,128)(2,1)}) %all-gather.5.cloned.1.call-update) | async-done | bytes 4194320 | tf_op jit(solution)/shard_map/all_gather | solution.py:67
  162.1 6.4 %copy.18 = bf16[8192,256]{0,1:T(8,128)(2,1)} copy(bf16[8192,256]{1,0:T(8,128)(2,1)} %all-gather.5.cloned.1.call-done) | data formatting | bytes 8388608
  168.6 12.4 %while.18 = (s32[]{:T(128)}, f32[2,1024]{1,0:T(2,128)S(1)}, f32[2,1024]{1,0:T(2,128)S(1)}, f32[2,1024,128]{2,1,0:T(8,128)S(1)}, s32[]{:T(128)}, /*index=5*/bf16[...) while((s32[]{:T(128)}, f32[2,1024]{1,0:T(2,128)S(1)}, ...), condition=%wide.region_9.10_spmd.clone, body=%wide.region_4.9_spmd.clone.sunk | while | flops 1115166720 | bytes 35352928 | solution.py:114
  168.6 11.9 %conditional.3 = ((f32[2,1024]{1,0:T(2,128)S(1)}, f32[2,1024]{1,0:T(2,128)S(1)}, f32[2,1024,128]{2,1,0:T(8,128)S(1)})) conditional(s32[]{:T(128)} %convert_element_type.57, (f32[2,1024]{1,0:T(2,128)S(1)}, f32[2,1024]{1,0:T(2,128)S(1)}, f32[2,1024,128]{2,1,0:T(8,128)S(1)}) %tuple.78, (s32[]{:T(128)}, s32[1024]{0:T(1024)S(1)}, s32[]{:T(128)}, ...), branch_computations={%region_5.5_spmd, %region_6.8_spmd} | conditional | flops 1115166720 | bytes 35348560 | solution.py:112
  168.7 1.3 constant_dynamic-slice_fusion
  170.6 2.6 fusion.6
  173.3 3.0 fusion.5
  176.3 4.2 %fusion.10 = f32[2,1024,128]{2,1,0:T(8,128)S(1)} fusion(bf16[1024,2,128]{0,2,1:T(8,128)(2,1)S(1)} %bitcast.65, f32[2,1024,1024]{2,1,0:T(8,128)S(1)} %get-tuple-element.336, f32[2,1024]{1,0:T(2,128)S(1)} %max.2, f32[2,1024]{1,0:T(2,128)S(1)} %dynamic-slice_bitcast_fusion, f32[2,1024]{1,0:T(2,128)S(1)} %get-tuple-element.230, ...), kind=kOutput, calls=%fused_computation.10 | convolution fusion | flops 552075264 | bytes 12091392 | tf_op jit(solution)/shard_map/while/body/eval_jaxpr/cond/branch_1_fun/hqk,khd->hqd/dot_general | solution.py:100
  181.4 7.1 %add_convert_fusion = bf16[1024,2048]{1,0:T(8,128)(2,1)} fusion(f32[1024,2048]{1,0:T(8,128)} %fusion.51, bf16[1024,256]{0,1:T(8,128)(2,1)S(1)} %bitcast.67, bf16[2048,2048]{1,0:T(8,128)(2,1)} %param.23, s32[]{:T(128)S(6)} %select_n.19), kind=kOutput, calls=%fused_computation.21 | convolution fusion | flops 1077936128 | bytes 14155780 | tf_op jit(solution)/shard_map/dot_general | solution.py:123
  188.5 126.7 %reduce-scatter.2.cloned.1.call-done = bf16[256,2048]{1,0:T(8,128)(2,1)} async-done(((bf16[1024,2048]{1,0:T(8,128)(2,1)}), bf16[256,2048]{1,0:T(8,128)(2,1)}) %reduce-scatter.2.cloned.1.call-update) | async-done | bytes 1048592 | tf_op jit(solution)/shard_map/reduce_scatter | solution.py:122
  (56 shorter events, 2.3 us)
Async XLA Ops:
  6.5 1.2 copy-start
  6.5 10.3 %copy-start.6 = (bf16[2048,256]{1,0:T(8,128)(2,1)S(1)}, bf16[2048,256]{1,0:T(8,128)(2,1)}, u32[]{:S(2)}) copy-start(bf16[2048,256]{1,0:T(8,128)(2,1)} %param.19) | copy-start | bytes 3145732
  6.5 81.9 %all-gather.3.cloned.1.call-start = ((), (), s32[]{:S(2)}) async-start(), calls=%async_computation.1 | async-start | bytes 4718592 | tf_op jit(solution)/shard_map/all_gather | solution.py:66
  12.0 8.4 %copy-start.7 = (bf16[2048,256]{1,0:T(8,128)(2,1)S(1)}, bf16[2048,256]{1,0:T(8,128)(2,1)}, u32[]{:S(2)}) copy-start(bf16[2048,256]{1,0:T(8,128)(2,1)} %param.18) | copy-start | bytes 3145732
  12.0 150.1 %all-gather.5.cloned.1.call-start = ((), (), s32[]{:S(2)}) async-start(), calls=%async_computation.2 | async-start | bytes 4718592 | tf_op jit(solution)/shard_map/all_gather | solution.py:67
  16.7 298.5 %reduce-scatter.2.cloned.1.call-start = ((), (), s32[]{:S(2)}) async-start(), calls=%async_computation.3 | async-start | bytes 5242880 | tf_op jit(solution)/shard_map/reduce_scatter | solution.py:122
  16.8 3.6 %copy-start.5 = (bf16[1024,2048]{1,0:T(8,128)(2,1)S(1)}, bf16[1024,2048]{1,0:T(8,128)(2,1)}, u32[]{:S(2)}) copy-start(bf16[1024,2048]{1,0:T(8,128)(2,1)} %param.14) | copy-start | bytes 12582916
  21.7 9.0 %copy-start.3 = (f32[31,256]{1,0:T(8,128)S(1)}, f32[31,256]{1,0:T(8,128)}, u32[]{:S(2)}) copy-start(f32[31,256]{1,0:T(8,128)} %param.20) | copy-start | bytes 95236
  21.7 9.1 %copy-start.2 = (f32[1024,2]{0,1:T(2,128)S(1)}, f32[1024,2]{0,1:T(2,128)}, u32[]{:S(2)}) copy-start(f32[1024,2]{0,1:T(2,128)} %param.22) | copy-start | bytes 24580
  21.7 40.9 %collective-permute-start = (bf16[30,256]{1,0:T(8,128)(2,1)S(1)}, bf16[30,256]{1,0:T(8,128)(2,1)S(1)}, u32[]{:S(2)}, u32[]{:S(2)}) collective-permute-start(bf16[30,256]{1,0:T(8,128)(2,1)S(1)} %slice.252), channel_id=1, source_target_pairs={{0,4},{4,8},{8,12},{12,16},{16,20},{20,24},{24,28},{1,5},{5,9},{9,... | collective-permute-start | bytes 46088 | tf_op jit(solution)/shard_map/ppermute | solution.py:14
  62.7 17.4 %copy-start.4 = (f32[256]{0:T(256)S(1)}, f32[256]{0:T(256)}, u32[]{:S(2)}) copy-start(f32[256]{0:T(256)} %param.21) | copy-start | bytes 3076
  181.4 133.8 %copy-start.1 = (bf16[2048,256]{1,0:T(8,128)(2,1)S(1)}, bf16[2048,256]{1,0:T(8,128)(2,1)}, u32[]{:S(2)}) copy-start(bf16[2048,256]{1,0:T(8,128)(2,1)} %param.16) | copy-start | bytes 3145732
Sparse Core Ops, SparseCore 0:
  12.1 76.2 all-gather.2
  90.6 71.4 all-gather.4
  188.6 126.5 reduce-scatter.1
where the time goes:
time: 322 us
  waiting for transfers between devices  196 us (61%)
  blocking collectives  44.5 us (14%)
  matrix products  37.3 us (12%)
  local copies, waits for them, and re-layouts  16.1 us (5%)
  between operations  13.3 us (4%)
  other arithmetic  8.6 us (3%)
  starting transfers between devices  4.96 us (2%)
    reduce_scatter x1, waiting for transfers between devices, on_device(): lax.psum_scatter((projected + jnp.dot(attn_rows, attn_weight, preferred_e...  127 us
    all_gather x1, waiting for transfers between devices, on_device(): piece_values = lax.all_gather(value_rows, 'sp', axis=0, tiled=True)  67.2 us
    all_gather x1, blocking collectives, on_device(): gates_all = lax.all_gather(log_forget, 'sp', axis=0, tiled=True)  31.8 us
    unnamed x19, local copies, waits for them, and re-layouts  14.3 us
    dot_general x1, matrix products, on_device(): jnp.dot(attn_rows, attn_weight, preferred_element_type=jnp.float32)  7.05 us
    psum x1, blocking collectives, on_device(): lax.psum(jnp.sum(centered * centered, axis=1), 'tp') / total_channels  6.63 us
  transfers between devices with their start and end apart: 4, of which 3 were waited for; matrix products, arithmetic and copies ran while one was open for 10% of the time, Pallas kernels for 0%

commit v1 on v0

--- a/solution.py
+++ b/solution.py
@@ -55,7 +55,6 @@
     value_rows = jnp.dot(inputs, w_value, preferred_element_type=jnp.float32).astype(jnp.bfloat16)
     query_heads = query_rows.reshape(tok_rows, heads_here, HEAD_DIM)
     own_gates = jnp.transpose(log_forget)
-    gates_all = lax.all_gather(log_forget, "sp", axis=0, tiled=True)
     score_scale = HEAD_DIM ** (-0.5)
     query_pos = row_start + jnp.arange(tok_rows, dtype=jnp.int32)
     start_state = (
@@ -63,7 +62,11 @@
         jnp.zeros((heads_here, tok_rows), jnp.float32),
         jnp.zeros((heads_here, tok_rows, HEAD_DIM), jnp.float32),
     )
-    piece_keys = lax.all_gather(key_rows, "sp", axis=0, tiled=True)
+    gates_all, piece_keys = jnp.split(
+        lax.all_gather(jnp.concatenate([log_forget, key_rows], axis=1), "sp", axis=0, tiled=True),
+        [log_forget.shape[1]],
+        axis=1,
+    )
     piece_values = lax.all_gather(value_rows, "sp", axis=0, tiled=True)
     block_rows = math.gcd(piece_keys.shape[0], tok_rows)
     shards = piece_keys.shape[0] // block_rows

time: 322 us -> 377 us (1.17)
  waiting for transfers between devices: 196 us -> 283 us
  blocking collectives: 44.5 us -> 12.4 us
    all_gather x1, waiting for transfers between devices: 2.45 us -> 122 us  [on_device(): lax.all_gather(jnp.concatenate([log_forget, key_rows], axis=1), 'sp', axi...]
    all_gather x1, waiting for transfers between devices: 67.2 us -> 34.9 us  [on_device(): piece_values = lax.all_gather(value_rows, 'sp', axis=0, tiled=True)]
    all_gather x1 -> x0, blocking collectives: 31.8 us -> none  [on_device(): gates_all = lax.all_gather(log_forget, 'sp', axis=0, tiled=True)]
    split x0 -> x2, local copies, waits for them, and re-layouts: none -> 7.3 us  [on_device(): jnp.split(lax.all_gather(jnp.concatenate([log_forget, key_rows], axis=1),...]
    unnamed x19 -> x18, local copies, waits for them, and re-layouts: 14.3 us -> 7.95 us
  transfers between devices with their start and end apart: 4 -> 4, of which waited for: 3 -> 3; matrix products, arithmetic and copies ran while one was open for 10% -> 8% of each run, Pallas kernels for 0% -> 0%
where the time goes in v1:
time: 377 us; the launch traced here: 376 us
  waiting for transfers between devices  283 us (75%)
  matrix products  35.2 us (9%)
  local copies, waits for them, and re-layouts  17 us (5%)
  between operations  13.3 us (4%)
  blocking collectives  12.4 us (3%)
  other arithmetic  9.86 us (3%)
  starting transfers between devices  4.99 us (1%)
    reduce_scatter x1, waiting for transfers between devices, on_device(): lax.psum_scatter((projected + jnp.dot(attn_rows, attn_weight, preferred_e...  126 us
    all_gather x1, waiting for transfers between devices, on_device(): lax.all_gather(jnp.concatenate([log_forget, key_rows], axis=1), 'sp', axi...  122 us
    all_gather x1, waiting for transfers between devices, on_device(): piece_values = lax.all_gather(value_rows, 'sp', axis=0, tiled=True)  34.9 us
    unnamed x18, local copies, waits for them, and re-layouts  7.95 us
  transfers between devices with their start and end apart: 4, of which 3 were waited for; matrix products, arithmetic and copies ran while one was open for 8% of the time, Pallas kernels for 0%

profile of v1, /device:TPU:0, one launch (start us, length us, event | category | flops | bytes accessed | tf_op | source)
XLA Modules:
  0.0 376.5 jit_solution(8271166624745839424)
XLA Ops:
  6.5 1.2 copy-done
  7.8 4.2 %convolution_convert_fusion = bf16[1024,256]{1,0:T(8,128)(2,1)} fusion(bf16[1024,2048]{1,0:T(8,128)(2,1)} %param.14, bf16[2048,256]{1,0:T(8,128)(2,1)S(1)} %copy-done), kind=kOutput, calls=%fused_computation.28 | convolution fusion | flops 1074003968 | bytes 5767168 | tf_op jit(solution)/shard_map/dot_general | solution.py:55
  12.1 3.9 %fusion.20 = f32[1024,256]{0,1:T(8,128)S(1)} fusion(bf16[1024,2048]{1,0:T(8,128)(2,1)} %param.14, bf16[2048,256]{1,0:T(8,128)(2,1)} %param.16), kind=kOutput, calls=%fused_computation.31 | convolution fusion | flops 1074266112 | bytes 6291456 | tf_op jit(solution)/shard_map/dot_general | solution.py:54
  15.9 1.2 pad_maximum_fusion
  17.3 3.6 fusion.18
  20.9 2.5 fusion.19
  23.5 4.9 %collective-permute-start = (bf16[30,256]{1,0:T(8,128)(2,1)S(1)}, bf16[30,256]{1,0:T(8,128)(2,1)S(1)}, u32[]{:S(2)}, u32[]{:S(2)}) collective-permute-start(bf16[30,256]{1,0:T(8,128)(2,1)S(1)} %slice.252), channel_id=1, source_target_pairs={{0,4},{4,8},{8,12},{12,16},{16,20},{20,24},{24,28},{1,5},{5,9},{9,... | collective-permute-start | bytes 46088 | tf_op jit(solution)/shard_map/ppermute | solution.py:14
  28.5 1.3 convolution_convert_fusion.1
  30.2 4.3 %fusion.61 = (f32[1024]{0:T(1024)S(1)}, f32[1024,256]{1,0:T(8,128)S(1)}) fusion(f32[1054,256]{1,0:T(8,128)S(1)} %maximum_convert_fusion, f32[256]{0:T(256)S(1)} %bitcast.99, f32[256]{0:T(256)S(1)} %bitcast.100, f32[256]{0:T(256)S(1)} %bitcast.71, f32[256]{0:T(256)S(1)} %bitcast.72, f32[256]{0:T(256)S(1)} %bitcast.73, f32[256]{0:T(256)S(1)} %bitcast.74, ...), kind=kLoop, calls=%fused_computation.110 | loop fusion | flops 16251904 | bytes 33590272 | tf_op jit(solution)/shard_map/reduce_sum | solution.py:47
  34.5 6.7 %psum.14 = f32[1024]{0:T(1024)S(1)} all-reduce(f32[1024]{0:T(1024)S(1)} %get-tuple-element.333), channel_id=1, replica_groups=mesh['sp'=8,'tp'=4] {'tp'}, use_global_device_ids=true, to_apply=%region_1.0 | all-reduce | flops 1024 | bytes 8192 | tf_op jit(solution)/shard_map/psum | solution.py:47
  41.6 5.7 %psum.15 = f32[1024]{0:T(1024)S(1)} all-reduce(f32[1024]{0:T(1024)S(1)} %multiply_reduce_fusion), channel_id=1, replica_groups=mesh['sp'=8,'tp'=4] {'tp'}, use_global_device_ids=true, to_apply=%region_3.0 | all-reduce | flops 1024 | bytes 8192 | tf_op jit(solution)/shard_map/psum | solution.py:49
  47.3 5.8 %fusion.52 = f32[1024,2048]{1,0:T(8,128)} fusion(bf16[2048,2048]{1,0:T(8,128)(2,1)} %param.23, s32[]{:T(128)S(6)} %select_n.18, f32[1024,256]{1,0:T(8,128)S(1)} %get-tuple-element.334, f32[256]{0:T(256)S(1)} %copy-done.4, f32[1024]{0:T(1024)S(1)} %add_rsqrt_fusion, f32[1024]{0:T(1024)S(1)} %broadcast_multiply_fusion), kind=kOutput, calls=%fused_computation.96 | convolution fusion | flops 1075838976 | bytes 10494980 | tf_op jit(solution)/shard_map/dot_general | solution.py:124
  53.1 34.9 %all-gather.5.cloned.1.call-done = bf16[8192,256]{1,0:T(8,128)(2,1)} async-done(((bf16[1024,256]{1,0:T(8,128)(2,1)}), bf16[8192,256]{1,0:T(8,128)(2,1)}) %all-gather.5.cloned.1.call-update) | async-done | bytes 4194320 | tf_op jit(solution)/shard_map/all_gather | solution.py:70
  88.0 6.4 %copy.18 = bf16[8192,256]{0,1:T(8,128)(2,1)} copy(bf16[8192,256]{1,0:T(8,128)(2,1)} %all-gather.5.cloned.1.call-done) | data formatting | bytes 8388608
  94.5 122.0 %all-gather.3.cloned.1.call-done = f32[8192,258]{0,1:T(8,128)} async-done(((f32[1024,258]{0,1:T(8,128)}), f32[8192,258]{0,1:T(8,128)}) %all-gather.3.cloned.1.call-update) | async-done | bytes 8454160 | tf_op jit(solution)/shard_map/all_gather | solution.py:66
  217.4 6.3 %split.8 = bf16[8192,256]{0,1:T(8,128)(2,1)} slice(f32[8192,258]{0,1:T(8,128)} %all-gather.3.cloned.1.call-done), slice={[0:8192], [2:258]} | slice | bytes 8388608 | tf_op jit(solution)/shard_map/split | solution.py:65
  223.8 12.4 %while.18 = (s32[]{:T(128)}, f32[2,1024]{1,0:T(2,128)S(1)}, f32[2,1024]{1,0:T(2,128)S(1)}, f32[2,1024,128]{2,1,0:T(8,128)S(1)}, s32[]{:T(128)}, /*index=5*/bf16[...) while((s32[]{:T(128)}, f32[2,1024]{1,0:T(2,128)S(1)}, ...), condition=%wide.region_9.10_spmd.clone, body=%wide.region_4.9_spmd.clone.sunk | while | flops 1115166720 | bytes 35352928 | solution.py:117
  223.8 11.9 %conditional.3 = ((f32[2,1024]{1,0:T(2,128)S(1)}, f32[2,1024]{1,0:T(2,128)S(1)}, f32[2,1024,128]{2,1,0:T(8,128)S(1)})) conditional(s32[]{:T(128)} %convert_element_type.64, (f32[2,1024]{1,0:T(2,128)S(1)}, f32[2,1024]{1,0:T(2,128)S(1)}, f32[2,1024,128]{2,1,0:T(8,128)S(1)}) %tuple.78, (s32[]{:T(128)}, s32[1024]{0:T(1024)S(1)}, s32[]{:T(128)}, ...), branch_computations={%region_5.5_spmd, %region_6.8_spmd} | conditional | flops 1115166720 | bytes 35348560 | solution.py:115
  223.9 1.3 constant_dynamic-slice_fusion
  225.8 2.6 fusion.6
  228.5 3.0 fusion.5
  231.5 4.2 %fusion.10 = f32[2,1024,128]{2,1,0:T(8,128)S(1)} fusion(bf16[1024,2,128]{0,2,1:T(8,128)(2,1)S(1)} %bitcast.65, f32[2,1024,1024]{2,1,0:T(8,128)S(1)} %get-tuple-element.336, f32[2,1024]{1,0:T(2,128)S(1)} %max.2, f32[2,1024]{1,0:T(2,128)S(1)} %dynamic-slice_bitcast_fusion, f32[2,1024]{1,0:T(2,128)S(1)} %get-tuple-element.230, ...), kind=kOutput, calls=%fused_computation.10 | convolution fusion | flops 552075264 | bytes 12091392 | tf_op jit(solution)/shard_map/while/body/eval_jaxpr/cond/branch_1_fun/hqk,khd->hqd/dot_general | solution.py:103
  236.7 7.0 %add_convert_fusion = bf16[1024,2048]{1,0:T(8,128)(2,1)} fusion(f32[1024,2048]{1,0:T(8,128)} %fusion.52, bf16[1024,256]{0,1:T(8,128)(2,1)S(1)} %bitcast.67, bf16[2048,2048]{1,0:T(8,128)(2,1)} %param.23, s32[]{:T(128)S(6)} %select_n.19), kind=kOutput, calls=%fused_computation.21 | convolution fusion | flops 1077936128 | bytes 14155780 | tf_op jit(solution)/shard_map/dot_general | solution.py:126
  243.7 126.2 %reduce-scatter.2.cloned.1.call-done = bf16[256,2048]{1,0:T(8,128)(2,1)} async-done(((bf16[1024,2048]{1,0:T(8,128)(2,1)}), bf16[256,2048]{1,0:T(8,128)(2,1)}) %reduce-scatter.2.cloned.1.call-update) | async-done | bytes 1048592 | tf_op jit(solution)/shard_map/reduce_scatter | solution.py:125
  (57 shorter events, 3.3 us)
Async XLA Ops:
  6.5 1.2 copy-start
  6.5 81.5 %all-gather.5.cloned.1.call-start = ((), (), s32[]{:S(2)}) async-start(), calls=%async_computation.2 | async-start | bytes 4718592 | tf_op jit(solution)/shard_map/all_gather | solution.py:70
  12.0 3.9 %copy-start.2 = (f32[1024,2]{0,1:T(2,128)S(1)}, f32[1024,2]{0,1:T(2,128)}, u32[]{:S(2)}) copy-start(f32[1024,2]{0,1:T(2,128)} %param.22) | copy-start | bytes 24580
  12.0 5.3 %copy-start.6 = (bf16[2048,256]{1,0:T(8,128)(2,1)S(1)}, bf16[2048,256]{1,0:T(8,128)(2,1)}, u32[]{:S(2)}) copy-start(bf16[2048,256]{1,0:T(8,128)(2,1)} %param.19) | copy-start | bytes 3145732
  12.0 204.4 %all-gather.3.cloned.1.call-start = ((), (), s32[]{:S(2)}) async-start(), calls=%async_computation.1 | async-start | bytes 9732096 | tf_op jit(solution)/shard_map/all_gather | solution.py:66
  17.2 11.2 %copy-start.3 = (f32[31,256]{1,0:T(8,128)S(1)}, f32[31,256]{1,0:T(8,128)}, u32[]{:S(2)}) copy-start(f32[31,256]{1,0:T(8,128)} %param.20) | copy-start | bytes 95236
  17.2 352.7 %reduce-scatter.2.cloned.1.call-start = ((), (), s32[]{:S(2)}) async-start(), calls=%async_computation.3 | async-start | bytes 5242880 | tf_op jit(solution)/shard_map/reduce_scatter | solution.py:125
  17.3 3.6 copy-start.5
  17.3 11.1 %copy-start.7 = (bf16[2048,256]{1,0:T(8,128)(2,1)S(1)}, bf16[2048,256]{1,0:T(8,128)(2,1)}, u32[]{:S(2)}) copy-start(bf16[2048,256]{1,0:T(8,128)(2,1)} %param.15) | copy-start | bytes 3145732
  23.5 6.6 %collective-permute-start = (bf16[30,256]{1,0:T(8,128)(2,1)S(1)}, bf16[30,256]{1,0:T(8,128)(2,1)S(1)}, u32[]{:S(2)}, u32[]{:S(2)}) collective-permute-start(bf16[30,256]{1,0:T(8,128)(2,1)S(1)} %slice.252), channel_id=1, source_target_pairs={{0,4},{4,8},{8,12},{12,16},{16,20},{20,24},{24,28},{1,5},{5,9},{9,... | collective-permute-start | bytes 46088 | tf_op jit(solution)/shard_map/ppermute | solution.py:14
  30.2 17.1 %copy-start.4 = (f32[256]{0:T(256)S(1)}, f32[256]{0:T(256)}, u32[]{:S(2)}) copy-start(f32[256]{0:T(256)} %param.21) | copy-start | bytes 3076
  236.7 133.3 %copy-start.1 = (bf16[2048,256]{1,0:T(8,128)(2,1)S(1)}, bf16[2048,256]{1,0:T(8,128)(2,1)}, u32[]{:S(2)}) copy-start(bf16[2048,256]{1,0:T(8,128)(2,1)} %param.17) | copy-start | bytes 3145732
Sparse Core Ops, SparseCore 0:
  12.1 75.8 all-gather.4
  90.2 126.1 all-gather.2
  243.8 126.0 reduce-scatter.1
